TPU v7x, 256 devices: a whole 4x4x8 slice. The times are simulated.
256 devices in a mesh: ep: 16 (over y, x), tp: 16 (over z, core).
Axes of the slice: x: 4, y: 4, z: 8, core: 2. Of those that a mesh axis runs over, the one named last changes fastest.
Arguments:
- tokens: bfloat16 [256, 2048], P('ep', 'tp'), may hold values from -6 to 6
- key_cache: bfloat16 [256, 16, 1024, 128], P('ep', 'tp'), may hold values from -1700 to 1700
- value_cache: bfloat16 [256, 16, 1024, 128], P('ep', 'tp'), may hold values from -6 to 6
- gate_totals: float32 [256, 16, 1024], P('ep', 'tp'), as said below
- lengths: int32 [256], P('ep'), may hold values from 128 to 1024
- attn_gain: float32 [2048], replicated, may hold values from 0.1 to 1.9
- w_query: bfloat16 [2048, 2048], P(None, 'tp'), may hold values from -0.125 to 0.125
- w_key: bfloat16 [2048, 2048], P(None, 'tp'), may hold values from -0.125 to 0.125
- w_value: bfloat16 [2048, 2048], P(None, 'tp'), may hold values from -0.125 to 0.125
- w_forget: bfloat16 [2048, 16], replicated, may hold values from -0.125 to 0.125
- forget_bias: float32 [16], replicated, may hold values from -3 to 0
- w_attn_out: bfloat16 [2048, 2048], P('tp'), may hold values from -0.1875 to 0.1875
- moe_gain: float32 [2048], replicated, may hold values from 0.1 to 1.9
- group_ids: int32 [256, 1], P('ep'), may hold values from 0 to 15; in each aligned block of 16 rows (0 to 15, 16 to 31, ...) at most 2 rows name the same one
- inner_ids: int32 [256, 2], P('ep'), may hold values from 0 to 3, all different within a row
- group_prob: float32 [256], P('ep'), may hold values from 0.2 to 1
- pair_logits: float32 [256, 2], P('ep'), may hold values from -6 to 6
- w_expert_gate: bfloat16 [16, 2048, 2048], P('ep', None, 'tp'), may hold values from -0.125 to 0.125
- w_expert_up: bfloat16 [16, 2048, 2048], P('ep', None, 'tp'), may hold values from -0.125 to 0.125
- w_expert_down: bfloat16 [16, 2048, 2048], P('ep', 'tp'), may hold values from -0.375 to 0.375
- w_dense_in: bfloat16 [2048, 2048], P(None, 'tp'), may hold values from -0.125 to 0.125
- w_dense_out: bfloat16 [2048, 2048], P('tp'), may hold values from -0.1875 to 0.1875
- dense_gate: float32 [2048], P('tp'), may hold values from -2 to 2
Outputs:
- layer_output: bfloat16 [256, 2048], P('ep', 'tp')
- new_keys: bfloat16 [256, 16, 128], P('ep', 'tp')
- new_values: bfloat16 [256, 16, 128], P('ep', 'tp')
- new_gates: float32 [256, 16], P('ep', 'tp')
Inputs may be any that keep to these rules, and one draw needn't show every extreme that they name: `group_ids`: within the 16 sequences of each index of ep (aligned blocks of rows), no group is named by more than 2 sequences, a bound that some block reaches. `inner_ids`: each row names 2 different experts of its group. `gate_totals`: along positions the values of each sequence and head never rise.
All inputs are finite; a program needn't handle non-finite values.
Results may differ from a plain program's by a relative error of at most 0.011.
Values may be sent and summed in bfloat16 or wider, within the bound.
A program may use at most 64 MiB of HBM per device.

v0:
```python
import jax
import jax.numpy as jnp
from jax import lax
from jax.sharding import PartitionSpec as P

FFE = 512
EPG = 4


EPS = 1e-06
FLOOR = -1e30


def split_up(array, dim, size):
    dims = array.shape
    pieces = array.reshape(*dims[:dim], size, dims[dim] // size, *dims[dim + 1 :])
    return jnp.moveaxis(pieces, dim, 0)


def sum_at_owner(array, axis, dim):
    size = lax.axis_size(axis)
    pieces = lax.all_to_all(split_up(array, dim, size), axis, 0, 0, tiled=True)
    return jnp.sum(pieces, axis=0)


def joined_along(pieces, dim):
    dims = list(pieces.shape[1:])
    dims[dim] *= pieces.shape[0]
    return jnp.moveaxis(pieces, 0, dim).reshape(dims)


def copy_for_each(array, axis):
    copies = jnp.broadcast_to(array, (lax.axis_size(axis), *array.shape))
    return lax.all_to_all(copies, axis, split_axis=0, concat_axis=0, tiled=True)


def gathered_copies(array, axis, dim):
    return joined_along(copy_for_each(array, axis), dim)


def side_by_side(arrays, axis, split_dim, concat_dim, along):
    both = jnp.concatenate(arrays, axis=along)
    filled, at, gathered = (
        lax.all_to_all(both, axis, split_axis=split_dim, concat_axis=concat_dim, tiled=True),
        0,
        [],
    )
    for a in arrays:
        gathered.append(lax.slice_in_dim(filled, at, at + a.shape[along], axis=along))
        at += a.shape[along]
    return tuple(gathered)


def sent_together(arrays, axis, dim, along):
    widths = [a.shape[along] for a in arrays]
    both = jnp.concatenate(arrays, axis=along)
    filled = sum_at_owner(both, axis, dim)
    return tuple(jnp.split(filled, [sum(widths[:k]) for k in range(1, len(widths))], axis=along))


def norm_rows(row_data, gain_vec):
    values = row_data.astype(jnp.float32)
    factor = lax.rsqrt(jnp.mean(values * values, axis=-1, keepdims=True) + EPS)
    return (values * factor * gain_vec).astype(jnp.bfloat16)


def head_norm(values):
    factor = lax.rsqrt(jnp.mean(values * values, axis=-1, keepdims=True) + EPS)
    return (values * factor).astype(jnp.bfloat16)


def attend(queries, fresh_key, fresh_value, key_cache, value_cache, gate_totals, lengths, current):
    score_scale = queries.shape[-1] ** (-0.5)
    scores = (
        jnp.einsum("shd,shld->shl", queries, key_cache, preferred_element_type=jnp.float32)
        * score_scale
    )
    scores = scores + current[:, :, None] - gate_totals
    entry_indices = jnp.arange(key_cache.shape[2])
    live_mask = (entry_indices[None, :] < lengths[:, None])[:, None, :]
    scores = jnp.where(live_mask, scores, FLOOR)
    own_score = (
        jnp.sum(queries.astype(jnp.float32) * fresh_key.astype(jnp.float32), axis=-1) * score_scale
    )
    peak = jnp.maximum(jnp.max(scores, axis=-1), own_score)
    expo_terms = jnp.where(live_mask, jnp.exp(scores - peak[:, :, None]), 0.0)
    own_expo = jnp.exp(own_score - peak)
    denom_sum = jnp.sum(expo_terms, axis=-1) + own_expo
    weights = (expo_terms / denom_sum[:, :, None]).astype(jnp.bfloat16)
    own_weight = (own_expo / denom_sum).astype(jnp.bfloat16)
    attended = jnp.einsum("shl,shld->shd", weights, value_cache, preferred_element_type=jnp.float32)
    attended = attended + own_weight.astype(jnp.float32)[:, :, None] * fresh_value.astype(
        jnp.float32
    )
    return attended.astype(jnp.bfloat16)


def body(
    tokens,
    key_cache,
    value_cache,
    gate_totals,
    lengths,
    attn_gain,
    w_query,
    w_key,
    w_value,
    w_forget,
    forget_bias,
    w_attn_out,
    moe_gain,
    group_ids,
    inner_ids,
    group_prob,
    pair_logits,
    w_expert_gate,
    w_expert_up,
    w_expert_down,
    w_dense_in,
    w_dense_out,
    dense_gate,
):
    gathered = lax.all_gather(tokens, "tp", axis=1, tiled=True)
    normed = norm_rows(gathered, attn_gain)
    seq_count = gathered.shape[0]
    heads_dev = key_cache.shape[1]
    head_dim = key_cache.shape[3]

    def project(weight):
        return jnp.dot(normed, weight, preferred_element_type=jnp.float32).reshape(
            seq_count, heads_dev, head_dim
        )

    queries = head_norm(project(w_query))
    new_keys = head_norm(project(w_key))
    new_values = project(w_value).astype(jnp.bfloat16)
    first_head = lax.axis_index("tp") * heads_dev
    forget_cols = lax.dynamic_slice_in_dim(w_forget, first_head, heads_dev, 1)
    forget_shift = lax.dynamic_slice_in_dim(forget_bias, first_head, heads_dev, 0)
    log_gate = jax.nn.log_sigmoid(
        jnp.dot(normed, forget_cols, preferred_element_type=jnp.float32) + forget_shift
    )
    entry_indices = jnp.arange(gate_totals.shape[2])
    at_last = (entry_indices[None, :] == (lengths - 1)[:, None])[:, None, :]
    new_gates = jnp.sum(jnp.where(at_last, gate_totals, 0.0), axis=2) + log_gate
    attended = attend(
        queries, new_keys, new_values, key_cache, value_cache, gate_totals, lengths, new_gates
    )
    partial_value = jnp.dot(
        attended.reshape(seq_count, heads_dev * head_dim),
        w_attn_out,
        preferred_element_type=jnp.float32,
    )
    piece_sum = sum_at_owner(partial_value, "tp", 1)
    own_residual = (tokens.astype(jnp.float32) + piece_sum).astype(jnp.bfloat16)
    moe_in = norm_rows(gathered_copies(own_residual, "tp", 1), moe_gain)
    groups = lax.axis_size("ep")
    capacity = max(2, 2 * seq_count // groups)
    first_share = jax.nn.sigmoid(pair_logits[:, 0] - pair_logits[:, 1])
    pair_share = group_prob[:, None] * jnp.stack([first_share, 1.0 - first_share], axis=1)
    inner_range = jnp.arange(EPG)
    spread = jnp.sum(
        jnp.where(inner_ids[:, :, None] == inner_range[None, None, :], pair_share[:, :, None], 0.0),
        axis=1,
    ).astype(jnp.bfloat16)
    choose = (group_ids == jnp.arange(groups)[None, :]).astype(jnp.int32)
    before = jnp.cumsum(choose, axis=0) - choose
    slot_of = group_ids[:, 0] * capacity + jnp.sum(before * choose, axis=1)
    slot_ids = jnp.arange(groups * capacity)
    send_map = (slot_of[None, :] == slot_ids[:, None]).astype(jnp.bfloat16)
    send_weights = jnp.dot(send_map, spread, preferred_element_type=jnp.float32).astype(
        jnp.bfloat16
    )
    send_rows = jnp.dot(send_map, moe_in, preferred_element_type=jnp.float32).astype(jnp.bfloat16)
    recv_rows, recv_weights = side_by_side((send_rows, send_weights), "ep", 0, 0, 1)
    dense_hidden = jax.nn.silu(
        jnp.dot(moe_in, w_dense_in, preferred_element_type=jnp.float32)
    ).astype(jnp.bfloat16)
    dense_part = jnp.dot(dense_hidden, w_dense_out, preferred_element_type=jnp.float32)
    hidden_dev = w_expert_gate.shape[2]
    expert_index = lax.axis_index("tp") * hidden_dev // FFE
    route_col = jnp.sum(
        jnp.where(inner_range[None, :] == expert_index, recv_weights.astype(jnp.float32), 0.0),
        axis=1,
    )
    gate_pre = jnp.dot(recv_rows, w_expert_gate[0], preferred_element_type=jnp.float32)
    up_pre = jnp.dot(recv_rows, w_expert_up[0], preferred_element_type=jnp.float32)
    hidden = (jax.nn.silu(gate_pre) * up_pre * route_col[:, None]).astype(jnp.bfloat16)
    expert_part = jnp.dot(hidden, w_expert_down[0], preferred_element_type=jnp.float32)
    expert_sum, dense_sum = sent_together((expert_part, dense_part), "tp", 1, 0)
    returned = lax.all_to_all(
        expert_sum.astype(jnp.bfloat16), "ep", split_axis=0, concat_axis=0, tiled=True
    )
    expert_out = lax.dot_general(
        send_map, returned, (((0,), (0,)), ((), ())), preferred_element_type=jnp.float32
    )
    layer_output = (
        own_residual.astype(jnp.float32) + expert_out + jax.nn.sigmoid(dense_gate) * dense_sum
    )
    return (layer_output.astype(jnp.bfloat16), new_keys, new_values, new_gates)


def solution(mesh):
    placed = (
        P("ep", "tp"),
        P("ep", "tp", None, None),
        P("ep", "tp", None, None),
        P("ep", "tp", None),
        P("ep"),
        P(),
        P(None, "tp"),
        P(None, "tp"),
        P(None, "tp"),
        P(),
        P(),
        P("tp", None),
        P(),
        P("ep", None),
        P("ep", None),
        P("ep"),
        P("ep", None),
        P("ep", None, "tp"),
        P("ep", None, "tp"),
        P("ep", "tp", None),
        P(None, "tp"),
        P("tp", None),
        P("tp"),
    )
    return jax.shard_map(
        body,
        mesh=mesh,
        in_specs=placed,
        out_specs=(P("ep", "tp"), P("ep", "tp", None), P("ep", "tp", None), P("ep", "tp")),
        check_vma=False,
    )
```

profile of v0, /device:TPU:1, one launch (start us, length us, event | category | flops | bytes accessed | tf_op | source)
XLA Modules:
  0.0 108.0 jit_solution(13230268292263461012)
XLA Ops:
  0.7 21.8 %all_gather.3 = bf16[16,2048]{1,0:T(8,128)(2,1)S(1)} all-gather(bf16[16,128]{1,0:T(8,128)(2,1)} %param.23), channel_id=1, replica_groups=mesh['ep'=16,'tp'=16] {'tp'}, dimensions={1}, use_global_device_ids=true | all-gather | bytes 69632 | tf_op jit(solution)/shard_map/all_gather | solution.py:123
  22.7 1.4 %multiply_reduce_fusion.1 = (f32[16]{0:T(128)S(1)}, f32[16,128]{1,0:T(8,128)S(1)}) fusion(bf16[2048,128]{1,0:T(8,128)(2,1)} %param.30, bf16[16,2048]{1,0:T(8,128)(2,1)S(1)} %all_gather.3, f32[2048]{0:T(1024)} %param.28, f32[16]{0:T(128)S(1)} %add_rsqrt_fusion.3), kind=kOutput, calls=%fused_computation.71 | convolution fusion | flops 8523760 | bytes 606336 | tf_op jit(solution)/shard_map/dot_general | solution.py:130
  24.1 1.4 %multiply_reduce_fusion.2 = (f32[16]{0:T(128)S(1)}, f32[16,128]{1,0:T(8,128)S(1)}) fusion(bf16[2048,128]{1,0:T(8,128)(2,1)} %param.29, bf16[16,2048]{1,0:T(8,128)(2,1)S(1)} %all_gather.3, f32[2048]{0:T(1024)} %param.28, f32[16]{0:T(128)S(1)} %add_rsqrt_fusion.3), kind=kOutput, calls=%fused_computation.74 | convolution fusion | flops 8523760 | bytes 606336 | tf_op jit(solution)/shard_map/dot_general | solution.py:130
  25.5 0.7 broadcast_add_fusion
  26.2 0.8 fusion.59
  27.0 3.4 %fusion.2 = f32[16,1,1024]{2,1,0:T(1,128)S(1)} fusion(bf16[16,1,1024,128]{3,2,1,0:T(8,128)(2,1)} %param.24, bf16[16,128,1]{1,0,2:T(8,128)(2,1)S(1)} %get-tuple-element.10), kind=kOutput, calls=%fused_computation.2 | convolution fusion | flops 4194304 | bytes 4263936 | tf_op jit(solution)/shard_map/shd,shld->shl/dot_general | solution.py:75
  30.4 0.6 dynamic_slice.7
  31.0 0.3 fusion.29
  31.3 1.6 %fusion.51 = f32[16]{0:T(128)S(1)} fusion(f32[16]{0:T(128)S(1)} %fusion.29, bf16[2048,16]{0,1:T(8,128)(2,1)} %param.32, s32[]{:T(128)S(6)} %select_n.34, f32[]{:T(128)} %bitcast.4, bf16[16,2048]{1,0:T(8,128)(2,1)S(1)} %all_gather.3, f32[2048]{0:T(1024)S(1)} %copy-done.8, f32[16]{0:T(128)S(1)} %add_rsqrt_fusion.3), kind=kOutput, calls=%fused_computation.85 | convolution fusion | flops 196768 | bytes 82628 | tf_op jit(solution)/shard_map/dot_general | solution.py:141
  33.0 0.3 fusion.74
  33.4 0.3 fusion.73
  33.7 0.2 convolution_convert_fusion.1
  34.0 0.3 copy.53
  34.3 3.0 %fusion = f32[16,1,128]{2,1,0:T(1,128)S(1)} fusion(bf16[16,1,1024,128]{3,2,1,0:T(8,128)(2,1)} %param.25, f32[16]{0:T(128)S(1)} %get-tuple-element.12, f32[16,1,1024]{2,1,0:T(1,128)S(1)} %get-tuple-element.7, f32[16]{0:T(128)S(1)} %multiply_maximum_fusion, s32[16]{0:T(128)S(1)} %copy-done.12), kind=kOutput, calls=%fused_computation | convolution fusion | flops 4276224 | bytes 4268224 | tf_op jit(solution)/shard_map/shl,shld->shd/dot_general | solution.py:91
  37.3 0.9 convolution_bitcast_fusion
  38.3 3.8 %all-to-all-start = ((f32[16,16,128]{2,1,0:T(8,128)}), f32[16,16,128]{2,1,0:T(8,128)S(1)}, u32[]{:S(2)}, u32[]{:S(2)}) async-start(f32[16,16,128]{2,1,0:T(8,128)} %convolution_bitcast_fusion), calls=%async_computation | async-start | bytes 262144 | tf_op jit(solution)/shard_map/all_to_all | solution.py:22
  42.5 8.5 %all-to-all-done = f32[16,16,128]{2,1,0:T(8,128)S(1)} async-done(((f32[16,16,128]{2,1,0:T(8,128)}), f32[16,16,128]{2,1,0:T(8,128)S(1)}, u32[]{:S(2)}, u32[]{:S(2)}) %all-to-all-start) | async-done | bytes 131104 | tf_op jit(solution)/shard_map/all_to_all | solution.py:22
  51.0 0.6 broadcast_in_dim.32
  51.6 3.4 %all-to-all-start.1 = ((bf16[16,16,128]{2,1,0:T(8,128)(2,1)}), bf16[16,16,128]{2,1,0:T(8,128)(2,1)S(1)}, u32[]{:S(2)}, u32[]{:S(2)}) async-start(bf16[16,16,128]{2,1,0:T(8,128)(2,1)} %broadcast_in_dim.32), calls=%async_computation.1 | async-start | bytes 131072 | tf_op jit(solution)/shard_map/all_to_all | solution.py:34
  55.3 7.2 %all-to-all-done.1 = bf16[16,16,128]{2,1,0:T(8,128)(2,1)S(1)} async-done(((bf16[16,16,128]{2,1,0:T(8,128)(2,1)}), bf16[16,16,128]{2,1,0:T(8,128)(2,1)S(1)}, u32[]{:S(2)}, u32[]{:S(2)}) %all-to-all-start.1) | async-done | bytes 65568 | tf_op jit(solution)/shard_map/all_to_all | solution.py:34
  62.6 0.2 convolution_convert_fusion
  62.9 0.7 all_to_all.27
  63.6 6.8 %all-to-all-start.2 = ((bf16[16,2,2052]{2,1,0:T(2,128)(2,1)}), bf16[16,2,2052]{2,1,0:T(2,128)(2,1)S(1)}, u32[]{:S(2)}, u32[]{:S(2)}) async-start(bf16[16,2,2052]{2,1,0:T(2,128)(2,1)} %all_to_all.27), calls=%async_computation.2 | async-start | bytes 278528 | tf_op jit(solution)/shard_map/all_to_all | solution.py:44
  70.4 0.4 fusion.44
  70.8 6.4 %all-to-all-done.2 = bf16[16,2,2052]{2,1,0:T(2,128)(2,1)S(1)} async-done(((bf16[16,2,2052]{2,1,0:T(2,128)(2,1)}), bf16[16,2,2052]{2,1,0:T(2,128)(2,1)S(1)}, u32[]{:S(2)}, u32[]{:S(2)}) %all-to-all-start.2) | async-done | bytes 131360 | tf_op jit(solution)/shard_map/all_to_all | solution.py:44
  77.5 0.2 fusion.14
  77.7 0.4 fusion.6
  78.1 18.6 %all_to_all.39 = f32[16,48,128]{2,1,0:T(8,128)S(1)} all-to-all(f32[16,48,128]{2,1,0:T(8,128)S(1)} %bitcast_bitcast_fusion), channel_id=1, replica_groups=mesh['ep'=16,'tp'=16] {'tp'}, dimensions={0} | all-to-all | bytes 786432 | tf_op jit(solution)/shard_map/all_to_all | solution.py:22
  96.8 0.6 split.15
  97.4 3.5 %all-to-all-start.4 = ((bf16[16,2,128]{2,1,0:T(2,128)(2,1)}), bf16[16,2,128]{2,1,0:T(2,128)(2,1)S(1)}, u32[]{:S(2)}, u32[]{:S(2)}) async-start(bf16[16,2,128]{2,1,0:T(2,128)(2,1)} %bitcast.19), calls=%async_computation.4 | async-start | bytes 16384 | tf_op jit(solution)/shard_map/all_to_all | solution.py:191
  100.9 6.3 %all-to-all-done.4 = bf16[16,2,128]{2,1,0:T(2,128)(2,1)S(1)} async-done(((bf16[16,2,128]{2,1,0:T(2,128)(2,1)}), bf16[16,2,128]{2,1,0:T(2,128)(2,1)S(1)}, u32[]{:S(2)}, u32[]{:S(2)}) %all-to-all-start.4) | async-done | bytes 8224 | tf_op jit(solution)/shard_map/all_to_all | solution.py:191
  107.3 0.8 fusion.8
  (66 shorter events, 1.4 us)
Async XLA Ops:
  0.6 77.0 %copy-start = (bf16[1,128,2048]{2,1,0:T(8,128)(2,1)S(1)}, bf16[1,128,2048]{2,1,0:T(8,128)(2,1)}, u32[]{:S(2)}) copy-start(bf16[1,128,2048]{2,1,0:T(8,128)(2,1)} %param.42) | copy-start | bytes 1572868
  0.6 30.7 %copy-start.8 = (f32[2048]{0:T(1024)S(1)}, f32[2048]{0:T(1024)}, u32[]{:S(2)}) copy-start(f32[2048]{0:T(1024)} %param.28) | copy-start | bytes 24580
  0.7 32.4 %copy-start.12 = (s32[16]{0:T(128)S(1)}, s32[16]{0:T(128)}, u32[]{:S(2)}) copy-start(s32[16]{0:T(128)} %param.27) | copy-start | bytes 196
  0.7 29.7 %copy-start.18 = (f32[16]{0:T(128)S(1)}, f32[16]{0:T(128)}, u32[]{:S(2)}) copy-start(f32[16]{0:T(128)} %param.33) | copy-start | bytes 196
  0.7 30.3 %copy-start.7 = (f32[16,1,1024]{2,1,0:T(1,128)S(1)}, f32[16,1,1024]{2,1,0:T(1,128)}, u32[]{:S(2)}) copy-start(f32[16,1,1024]{2,1,0:T(1,128)} %param.26) | copy-start | bytes 196612
  0.7 33.0 %copy-start.1 = (bf16[2048,128]{1,0:T(8,128)(2,1)S(1)}, bf16[2048,128]{1,0:T(8,128)(2,1)}, u32[]{:S(2)}) copy-start(bf16[2048,128]{1,0:T(8,128)(2,1)} %param.31) | copy-start | bytes 1572868
  0.7 33.3 %copy-start.2 = (bf16[128,2048]{1,0:T(8,128)(2,1)S(1)}, bf16[128,2048]{1,0:T(8,128)(2,1)}, u32[]{:S(2)}) copy-start(bf16[128,2048]{1,0:T(8,128)(2,1)} %param.34) | copy-start | bytes 1572868
  30.4 11.7 %copy-start.13 = (s32[16,1]{0,1:T(1,128)S(1)}, s32[16,1]{0,1:T(1,128)}, u32[]{:S(2)}) copy-start(s32[16,1]{0,1:T(1,128)} %param.36) | copy-start | bytes 196
  30.4 12.0 %copy-start.15 = (f32[16,2]{0,1:T(2,128)S(1)}, f32[16,2]{0,1:T(2,128)}, u32[]{:S(2)}) copy-start(f32[16,2]{0,1:T(2,128)} %param.39) | copy-start | bytes 388
  30.4 12.0 %copy-start.17 = (f32[16]{0:T(128)S(1)}, f32[16]{0:T(128)}, u32[]{:S(2)}) copy-start(f32[16]{0:T(128)} %param.38) | copy-start | bytes 196
  30.4 12.1 %copy-start.14 = (s32[16,2]{0,1:T(2,128)S(1)}, s32[16,2]{0,1:T(2,128)}, u32[]{:S(2)}) copy-start(s32[16,2]{0,1:T(2,128)} %param.37) | copy-start | bytes 388
  30.4 20.6 %copy-start.11 = (bf16[16,128]{1,0:T(8,128)(2,1)S(1)}, bf16[16,128]{1,0:T(8,128)(2,1)}, u32[]{:S(2)}) copy-start(bf16[16,128]{1,0:T(8,128)(2,1)} %param.23) | copy-start | bytes 12292
  30.4 32.2 %copy-start.9 = (f32[2048]{0:T(1024)S(1)}, f32[2048]{0:T(1024)}, u32[]{:S(2)}) copy-start(f32[2048]{0:T(1024)} %param.35) | copy-start | bytes 24580
  32.9 29.9 %copy-start.16 = (f32[16]{0:T(128)}, f32[16]{0:T(128)S(1)}, u32[]{:S(2)}) copy-start(f32[16]{0:T(128)S(1)} %fusion.51) | copy-start | bytes 196
  34.0 36.8 %copy-start.10 = (bf16[16,128]{1,0:T(8,128)(2,1)}, bf16[16,128]{1,0:T(8,128)(2,1)S(1)}, u32[]{:S(2)}) copy-start(bf16[16,128]{1,0:T(8,128)(2,1)S(1)} %convolution_convert_fusion.1) | copy-start | bytes 12292
  34.0 36.4 %copy-start.3 = (bf16[128,2048]{1,0:T(8,128)(2,1)S(1)}, bf16[128,2048]{1,0:T(8,128)(2,1)}, u32[]{:S(2)}) copy-start(bf16[128,2048]{1,0:T(8,128)(2,1)} %param.44) | copy-start | bytes 1572868
  34.0 36.4 %copy-start.4 = (bf16[2048,128]{1,0:T(8,128)(2,1)S(1)}, bf16[2048,128]{1,0:T(8,128)(2,1)}, u32[]{:S(2)}) copy-start(bf16[2048,128]{1,0:T(8,128)(2,1)} %param.43) | copy-start | bytes 1572868
  34.3 43.2 %copy-start.5 = (bf16[1,2048,128]{2,1,0:T(8,128)(2,1)S(1)}, bf16[1,2048,128]{2,1,0:T(8,128)(2,1)}, u32[]{:S(2)}) copy-start(bf16[1,2048,128]{2,1,0:T(8,128)(2,1)} %param.40) | copy-start | bytes 1572868
  34.3 43.4 %copy-start.6 = (bf16[1,2048,128]{2,1,0:T(8,128)(2,1)S(1)}, bf16[1,2048,128]{2,1,0:T(8,128)(2,1)}, u32[]{:S(2)}) copy-start(bf16[1,2048,128]{2,1,0:T(8,128)(2,1)} %param.41) | copy-start | bytes 1572868
  37.3 63.6 %copy-start.19 = (f32[128]{0:T(128)S(1)}, f32[128]{0:T(128)}, u32[]{:S(2)}) copy-start(f32[128]{0:T(128)} %param.45) | copy-start | bytes 1540
  38.3 12.7 %all-to-all-start = ((f32[16,16,128]{2,1,0:T(8,128)}), f32[16,16,128]{2,1,0:T(8,128)S(1)}, u32[]{:S(2)}, u32[]{:S(2)}) async-start(f32[16,16,128]{2,1,0:T(8,128)} %convolution_bitcast_fusion), calls=%async_computation | async-start | bytes 262144 | tf_op jit(solution)/shard_map/all_to_all | solution.py:22
  51.6 10.9 %all-to-all-start.1 = ((bf16[16,16,128]{2,1,0:T(8,128)(2,1)}), bf16[16,16,128]{2,1,0:T(8,128)(2,1)S(1)}, u32[]{:S(2)}, u32[]{:S(2)}) async-start(bf16[16,16,128]{2,1,0:T(8,128)(2,1)} %broadcast_in_dim.32), calls=%async_computation.1 | async-start | bytes 131072 | tf_op jit(solution)/shard_map/all_to_all | solution.py:34
  63.6 13.6 %all-to-all-start.2 = ((bf16[16,2,2052]{2,1,0:T(2,128)(2,1)}), bf16[16,2,2052]{2,1,0:T(2,128)(2,1)S(1)}, u32[]{:S(2)}, u32[]{:S(2)}) async-start(bf16[16,2,2052]{2,1,0:T(2,128)(2,1)} %all_to_all.27), calls=%async_computation.2 | async-start | bytes 278528 | tf_op jit(solution)/shard_map/all_to_all | solution.py:44
  97.4 9.9 %all-to-all-start.4 = ((bf16[16,2,128]{2,1,0:T(2,128)(2,1)}), bf16[16,2,128]{2,1,0:T(2,128)(2,1)S(1)}, u32[]{:S(2)}, u32[]{:S(2)}) async-start(bf16[16,2,128]{2,1,0:T(2,128)(2,1)} %bitcast.19), calls=%async_computation.4 | async-start | bytes 16384 | tf_op jit(solution)/shard_map/all_to_all | solution.py:191
where the time goes:
time: 109 us; the launch traced here: 108 us
  blocking collectives  40.5 us (37%)
  waiting for transfers between devices  28.5 us (26%)
  starting transfers between devices  17.4 us (16%)
  matrix products  14.1 us (13%)
  other arithmetic  3.35 us (3%)
  local copies, waits for them, and re-layouts  3.12 us (3%)
    all_gather x1, blocking collectives, body(): gathered = lax.all_gather(tokens, 'tp', axis=1, tiled=True)  21.8 us
    all_to_all x1, blocking collectives, sum_at_owner(): pieces = lax.all_to_all(split_up(array, dim, size), axis, 0, 0, tiled=True)  18.6 us
    all_to_all x1, waiting for transfers between devices, sum_at_owner(): pieces = lax.all_to_all(split_up(array, dim, size), axis, 0, 0, tiled=True)  8.5 us
    all_to_all x1, waiting for transfers between devices, copy_for_each(): return lax.all_to_all(copies, axis, split_axis=0, concat_axis=0, tiled=True)  7.21 us
    all_to_all x1, starting transfers between devices, side_by_side(): lax.all_to_all(both, axis, split_axis=split_dim, concat_axis=concat_dim,...  6.75 us
    all_to_all x1, waiting for transfers between devices, side_by_side(): lax.all_to_all(both, axis, split_axis=split_dim, concat_axis=concat_dim,...  6.44 us
    all_to_all x1, waiting for transfers between devices, body(): lax.all_to_all(expert_sum.astype(jnp.bfloat16), 'ep', split_axis=0, conca...  6.35 us
    all_to_all x1, starting transfers between devices, sum_at_owner(): pieces = lax.all_to_all(split_up(array, dim, size), axis, 0, 0, tiled=True)  3.81 us
  transfers between devices with their start and end apart: 4, of which 4 were waited for; matrix products, arithmetic and copies ran while one was open for 1% of the time, Pallas kernels for 0%

commit v1 on v0

v1 whole, which is shorter than its diff:
```python
import jax
import jax.numpy as jnp
from jax import lax
from jax.experimental import pallas as pl
from jax.experimental.pallas import tpu as pltpu
from jax.sharding import PartitionSpec as P

EPS = 1e-06
FLOOR = -1e30
MESH = pl.DeviceIdType.MESH
N = 16
HD = 128
D = N * HD
L = 1024
FFE = 512
KB = D // 256
F32 = jnp.float32
BF = jnp.bfloat16
TP_ORDER = (8, 9, 7, 6, 10, 5, 11, 4, 12, 3, 13, 2, 14, 15, 1)
EP_ORDER = (10, 5, 15, 6, 9, 2, 8, 11, 14, 7, 13, 1, 3, 4, 12)


def iota(shape, dim):
    return lax.broadcasted_iota(jnp.int32, shape, dim)


def dot(a, b, dims=((1,), (0,))):
    return lax.dot_general(a, b, (dims, ((), ())), preferred_element_type=F32)


def rms(values):
    return lax.rsqrt(jnp.mean(values * values, axis=-1, keepdims=True) + EPS)


def sigmoid(x):
    return 1.0 / (1.0 + jnp.exp(-x))


def column_of(row):
    wide = jnp.broadcast_to(row, (N, N))
    same = iota((N, N), 0) == iota((N, N), 1)
    return jnp.sum(jnp.where(same, wide, jnp.zeros_like(wide)), axis=1, keepdims=True)


def kernel(
    tokens, key_cache, value_cache, gate_totals, lengths, attn_gain, w_query, w_key, w_value,
    w_forget, forget_bias, w_attn_out, moe_gain, group_ids, inner_ids, group_prob, pair_logits,
    w_gate, w_up, w_down, w_din, w_dout, dense_gate,
    o_layer, o_keys, o_values, o_gates,
    k_v, v_v, wqkv, wf, wo, wgu, wdn, wdi, wdo, gt_v, len_v, ag_v, fb_v, mg_v, gid_v, inn_v,
    gp_v, pl_v, tok_all, dg_all, p_v, pt_v, part2, recv2, res_all, send4, recv4, dpart,
    send5, recv5, part6, recv6, keys_v, vals_v, gates_v, lay_v,
    lsem, ssem, rsem, osem,
):
    ep = lax.axis_index("ep")
    tp = lax.axis_index("tp")
    tcol = pl.ds(pl.multiple_of(tp * HD, HD), HD)
    erow = pl.ds(pl.multiple_of(ep * N, N), N)

    barrier = pltpu.get_barrier_semaphore()
    for off in range(1, N):
        pl.semaphore_signal(
            barrier, inc=1, device_id={"tp": lax.rem(tp + off, N)}, device_id_type=MESH
        )
        pl.semaphore_signal(
            barrier, inc=1, device_id={"ep": lax.rem(ep + off, N)}, device_id_type=MESH
        )

    count = [0]

    def local(src, dst):
        copy = pltpu.make_async_copy(src, dst, lsem.at[count[0]])
        count[0] += 1
        copy.start()
        return copy

    c_tok = local(tokens, tok_all.at[:, tcol])
    c_dg = local(dense_gate, dg_all.at[:, tcol])
    c_route = [
        local(group_ids, gid_v), local(inner_ids, inn_v), local(group_prob, gp_v),
        local(pair_logits, pl_v),
    ]
    c_small = [
        local(attn_gain, ag_v), local(lengths, len_v), local(forget_bias, fb_v),
        local(gate_totals, gt_v),
    ]
    c_qkv = [
        local(w_query, wqkv.at[:, 0:HD]), local(w_key, wqkv.at[:, HD : 2 * HD]),
        local(w_value, wqkv.at[:, 2 * HD : 3 * HD]), local(w_forget, wf),
    ]
    c_k = [local(key_cache.at[s, 0], k_v.at[:, s * HD : (s + 1) * HD]) for s in range(N)]
    c_v = [local(value_cache.at[s, 0], v_v.at[:, s * HD : (s + 1) * HD]) for s in range(N)]
    c_wo = local(w_attn_out, wo)
    c_mg = local(moe_gain, mg_v)
    c_dense = [local(w_din, wdi), local(w_dout, wdo)]
    c_expert = [
        local(w_gate.at[0], wgu.at[:, 0:HD]), local(w_up.at[0], wgu.at[:, HD : 2 * HD]),
        local(w_down.at[0], wdn),
    ]

    sends = []

    def push(phase, axis, order, src_of, dst):
        me = tp if axis == "tp" else ep
        for n, off in enumerate(order):
            peer = lax.rem(me + off, N)
            copy = pltpu.make_async_remote_copy(
                src_ref=src_of(peer),
                dst_ref=dst,
                send_sem=ssem.at[phase, n],
                recv_sem=rsem.at[phase, me],
                device_id={axis: peer},
                device_id_type=MESH,
            )
            copy.start()
            sends.append(copy)

    def arrive(phase, axis, order, dst_of):
        me = tp if axis == "tp" else ep
        for n, off in reversed(list(enumerate(order))):
            peer = lax.rem(me + off, N)
            pltpu.make_async_remote_copy(
                src_ref=dst_of(peer),
                dst_ref=dst_of(peer),
                send_sem=ssem.at[phase, n],
                recv_sem=rsem.at[phase, peer],
                device_id={axis: peer},
                device_id_type=MESH,
            ).wait_recv()

    def tp_cols(ref):
        return lambda peer: ref.at[:, pl.ds(pl.multiple_of(peer * HD, HD), HD)]

    def ep_rows(ref):
        return lambda peer: ref.at[pl.ds(pl.multiple_of(peer * N, N), N), :]

    def slots(ref):
        return lambda peer: ref.at[peer]

    for copy in c_route:
        copy.wait()
    gid = gid_v[...]
    choose = (gid == iota((N, N), 1)).astype(F32)
    lower = (iota((N, N), 1) < iota((N, N), 0)).astype(F32)
    before = dot(lower.astype(BF), choose.astype(BF))
    slot_of = gid * 2 + jnp.sum(before * choose, axis=1, keepdims=True).astype(jnp.int32)
    first = sigmoid(pl_v[:, 0:1] - pl_v[:, 1:2])
    prob = column_of(gp_v[...])
    share0, share1 = prob * first, prob * (1.0 - first)
    expert = tp * HD // FFE
    inner = inn_v[...]
    spread = jnp.where(inner[:, 0:1] == expert, share0, 0.0) + jnp.where(
        inner[:, 1:2] == expert, share1, 0.0
    )
    spread = spread.astype(BF).astype(F32)
    spread_k = jnp.concatenate([spread] * KB, axis=0)
    slot_k = jnp.concatenate([slot_of] * KB, axis=0)
    rows, cols = iota((KB * N, 256), 0), iota((KB * N, 256), 1)
    pt = ((slot_k == cols // KB) & (rows // N == lax.rem(cols, KB))).astype(F32)
    pt_v[...] = pt.astype(BF)
    p_v[...] = pt.T.astype(BF)

    c_tok.wait()
    c_dg.wait()
    pl.semaphore_wait(barrier, 2 * (N - 1))
    push(0, "tp", TP_ORDER, lambda peer: tok_all.at[:, tcol], tok_all.at[:, tcol])
    push(1, "tp", TP_ORDER, lambda peer: dg_all.at[:, tcol], dg_all.at[:, tcol])

    for copy in c_small + c_qkv:
        copy.wait()
    length = column_of(len_v[...])
    arrive(0, "tp", TP_ORDER, tp_cols(tok_all))

    toks = tok_all[...].astype(F32)
    normed = (toks * rms(toks) * ag_v[...]).astype(BF)
    qkv = dot(normed, wqkv[...])
    fg = dot(normed, wf[...])
    zq, zk = qkv[:, 0:HD], qkv[:, HD : 2 * HD]
    q = (zq * rms(zq)).astype(BF)
    new_k = (zk * rms(zk)).astype(BF)
    new_v = qkv[:, 2 * HD : 3 * HD].astype(BF)
    keys_v[...] = new_k
    vals_v[...] = new_v
    o_copies = [
        pltpu.make_async_copy(keys_v, o_keys, osem.at[0]),
        pltpu.make_async_copy(vals_v, o_values, osem.at[1]),
    ]
    for copy in o_copies:
        copy.start()
    pre = fg + fb_v[...]
    pre = jnp.sum(jnp.where(iota((N, N), 1) == tp, pre, 0.0), axis=1, keepdims=True)
    log_gate = jnp.minimum(pre, 0.0) - jnp.log(1.0 + jnp.exp(-jnp.abs(pre)))
    gt = gt_v[...].reshape(N, L)
    entry = iota((N, L), 1)
    last = jnp.sum(jnp.where(entry == length - 1, gt, 0.0), axis=1, keepdims=True)
    current = last + log_gate
    gates_v[...] = current
    c_gates = pltpu.make_async_copy(gates_v, o_gates, osem.at[2])
    c_gates.start()
    o_copies.append(c_gates)

    seq = iota((N, HD), 0)
    zero = jnp.zeros_like(q)
    q_wide = jnp.concatenate([jnp.where(seq == s, q, zero) for s in range(N)], axis=1)
    for copy in c_k:
        copy.wait()
    scale = HD ** (-0.5)
    scores = jnp.concatenate(
        [dot(q_wide, k_v[c : c + 256, :], ((1,), (1,))) for c in range(0, L, 256)], axis=1
    )
    scores = scores * scale + current - gt
    live = entry < length
    scores = jnp.where(live, scores, FLOOR)
    own = jnp.sum(q.astype(F32) * new_k.astype(F32), axis=1, keepdims=True) * scale
    peak = jnp.maximum(jnp.max(scores, axis=1, keepdims=True), own)
    expo = jnp.where(live, jnp.exp(scores - peak), 0.0)
    own_expo = jnp.exp(own - peak)
    denom = jnp.sum(expo, axis=1, keepdims=True) + own_expo
    weights = (expo / denom).astype(BF)
    own_weight = (own_expo / denom).astype(BF).astype(F32)
    for copy in c_v:
        copy.wait()
    attended = own_weight * new_v.astype(F32)
    for s in range(0, N, 2):
        both = dot(weights, v_v[:, s * HD : (s + 2) * HD])
        attended += jnp.where(seq == s, both[:, 0:HD], 0.0)
        attended += jnp.where(seq == s + 1, both[:, HD : 2 * HD], 0.0)
    attended = attended.astype(BF)

    c_wo.wait()
    part2[...] = dot(attended, wo[...]).astype(BF)
    push(2, "tp", TP_ORDER, tp_cols(part2), recv2.at[tp])
    recv2[tp] = part2[:, tcol]
    own_tok = tok_all[:, tcol].astype(F32)
    arrive(2, "tp", TP_ORDER, slots(recv2))
    residual = (own_tok + jnp.sum(recv2[...].astype(F32), axis=0)).astype(BF)
    res_all[:, tcol] = residual
    push(3, "tp", TP_ORDER, lambda peer: res_all.at[:, tcol], res_all.at[:, tcol])
    c_mg.wait()
    arrive(1, "tp", TP_ORDER, tp_cols(dg_all))
    dense_scale = sigmoid(dg_all[...])
    for copy in c_dense + c_expert:
        copy.wait()
    arrive(3, "tp", TP_ORDER, tp_cols(res_all))

    res = res_all[...].astype(F32)
    moe_in = (res * rms(res) * mg_v[...]).astype(BF)
    blocks = jnp.concatenate([moe_in[:, k * 256 : (k + 1) * 256] for k in range(KB)], axis=0)
    send4[...] = dot(p_v[...], blocks).astype(BF)
    push(4, "ep", EP_ORDER, ep_rows(send4), recv4.at[erow, :])
    recv4[erow, :] = send4[erow, :]

    hidden = dot(moe_in, wdi[...])
    hidden = (hidden * sigmoid(hidden)).astype(BF)
    dense = dot(hidden, wdo[...]) * dense_scale
    for k in range(KB):
        dpart[k * N : (k + 1) * N, :] = dense[:, k * 256 : (k + 1) * 256]

    rows, cols = iota((256, 256), 0), iota((256, 256), 1)
    regroup = (lax.rem(rows, 32) * KB + rows // 32 == cols).astype(F32).astype(BF)
    ungroup = (lax.rem(cols, 32) * KB + cols // 32 == rows).astype(F32).astype(BF)
    arrive(4, "ep", EP_ORDER, ep_rows(recv4))
    xs = dot(regroup, recv4[...]).astype(BF)
    x = jnp.concatenate([xs[k * 32 : (k + 1) * 32, :] for k in range(KB)], axis=1)
    gu = dot(x, wgu[...])
    g, u = gu[:, 0:HD], gu[:, HD : 2 * HD]
    h = (g * sigmoid(g) * u).astype(BF)
    y = dot(h, wdn[...]).astype(BF)
    ys = jnp.concatenate([y[:, k * 256 : (k + 1) * 256] for k in range(KB)], axis=0)
    send5[...] = dot(ungroup, ys).astype(BF)
    push(5, "ep", EP_ORDER, ep_rows(send5), recv5.at[erow, :])
    recv5[erow, :] = send5[erow, :]
    arrive(5, "ep", EP_ORDER, ep_rows(recv5))

    total = (dot(pt_v[...], recv5[...]) * spread_k + dpart[...]).astype(BF)
    for t in range(N):
        k, half = t // 2, t % 2
        part6[t] = total[k * N : (k + 1) * N, half * HD : (half + 1) * HD]
    push(6, "tp", TP_ORDER, slots(part6), recv6.at[tp])
    recv6[tp] = part6[tp]
    own_res = res_all[:, tcol].astype(F32)
    arrive(6, "tp", TP_ORDER, slots(recv6))
    lay_v[...] = (own_res + jnp.sum(recv6[...].astype(F32), axis=0)).astype(BF)
    c_lay = pltpu.make_async_copy(lay_v, o_layer, osem.at[3])
    c_lay.start()
    o_copies.append(c_lay)
    for copy in sends:
        copy.wait_send()
    for copy in o_copies:
        copy.wait()


def body(
    tokens, key_cache, value_cache, gate_totals, lengths, attn_gain, w_query, w_key, w_value,
    w_forget, forget_bias, w_attn_out, moe_gain, group_ids, inner_ids, group_prob, pair_logits,
    w_expert_gate, w_expert_up, w_expert_down, w_dense_in, w_dense_out, dense_gate,
):
    any_space = pl.BlockSpec(memory_space=pl.ANY)
    vmem = pltpu.VMEM
    outs = pl.pallas_call(
        kernel,
        out_shape=(
            jax.ShapeDtypeStruct((N, HD), BF),
            jax.ShapeDtypeStruct((N, HD), BF),
            jax.ShapeDtypeStruct((N, HD), BF),
            jax.ShapeDtypeStruct((N, 1), F32),
        ),
        in_specs=[any_space] * 23,
        out_specs=[any_space] * 4,
        scratch_shapes=[
            vmem((L, D), BF), vmem((L, D), BF), vmem((D, 3 * HD), BF), vmem((D, N), BF),
            vmem((HD, D), BF), vmem((D, 2 * HD), BF), vmem((HD, D), BF), vmem((D, HD), BF),
            vmem((HD, D), BF), vmem((N, 1, L), F32), vmem((1, N), jnp.int32), vmem((1, D), F32),
            vmem((1, N), F32), vmem((1, D), F32), vmem((N, 1), jnp.int32),
            vmem((N, 2), jnp.int32), vmem((1, N), F32), vmem((N, 2), F32),
            vmem((N, D), BF), vmem((1, D), F32), vmem((256, KB * N), BF), vmem((KB * N, 256), BF),
            vmem((N, D), BF), vmem((N, N, HD), BF), vmem((N, D), BF), vmem((256, 256), BF),
            vmem((256, 256), BF), vmem((KB * N, 256), F32), vmem((256, 256), BF),
            vmem((256, 256), BF), vmem((N, N, HD), BF), vmem((N, N, HD), BF),
            vmem((N, HD), BF), vmem((N, HD), BF), vmem((N, 1), F32), vmem((N, HD), BF),
            pltpu.SemaphoreType.DMA((64,)), pltpu.SemaphoreType.DMA((7, N)),
            pltpu.SemaphoreType.DMA((7, N)), pltpu.SemaphoreType.DMA((4,)),
        ],
        compiler_params=pltpu.CompilerParams(
            collective_id=0, has_side_effects=True, vmem_limit_bytes=48 * 1024 * 1024
        ),
    )(
        tokens, key_cache, value_cache, gate_totals, lengths.reshape(1, N),
        attn_gain.reshape(1, D), w_query, w_key, w_value, w_forget, forget_bias.reshape(1, N),
        w_attn_out, moe_gain.reshape(1, D), group_ids, inner_ids, group_prob.reshape(1, N),
        pair_logits, w_expert_gate, w_expert_up, w_expert_down, w_dense_in, w_dense_out,
        dense_gate.reshape(1, HD),
    )
    layer, keys, values, gates = outs
    return (layer, keys.reshape(N, 1, HD), values.reshape(N, 1, HD), gates)


def solution(mesh):
    placed = (
        P("ep", "tp"),
        P("ep", "tp", None, None),
        P("ep", "tp", None, None),
        P("ep", "tp", None),
        P("ep"),
        P(),
        P(None, "tp"),
        P(None, "tp"),
        P(None, "tp"),
        P(),
        P(),
        P("tp", None),
        P(),
        P("ep", None),
        P("ep", None),
        P("ep"),
        P("ep", None),
        P("ep", None, "tp"),
        P("ep", None, "tp"),
        P("ep", "tp", None),
        P(None, "tp"),
        P("tp", None),
        P("tp"),
    )
    return jax.shard_map(
        body,
        mesh=mesh,
        in_specs=placed,
        out_specs=(P("ep", "tp"), P("ep", "tp", None), P("ep", "tp", None), P("ep", "tp")),
        check_vma=False,
    )
```

time: 109 us -> 68.2 us (0.63)
  Pallas kernels: 0 us -> 46.1 us
  blocking collectives: 40.5 us -> 0 us
  waiting for transfers between devices: 28.5 us -> 0 us
  local copies, waits for them, and re-layouts: 3.12 us -> 20.6 us
  starting transfers between devices: 17.4 us -> 0 us
  matrix products: 14.1 us -> 0 us
  other arithmetic: 3.35 us -> 0 us
    pallas_call x0 -> x1, Pallas kernels: none -> 46.1 us  [body(): pl.pallas_call(kernel, out_shape=(jax.ShapeDtypeStruct((N, HD), BF), jax....]
    all_to_all x4 -> x0, waiting for transfers between devices: 28.5 us -> none  [the longest x1 8.5 us: sum_at_owner(): pieces = lax.all_to_all(split_up(array, dim, size), axis, 0, 0, tiled=True)]
    all_gather x1 -> x0, blocking collectives: 21.8 us -> none  [body(): gathered = lax.all_gather(tokens, 'tp', axis=1, tiled=True)]
    unnamed x40 -> x42, local copies, waits for them, and re-layouts: 0.12 us -> 20.6 us
    all_to_all x1 -> x0, blocking collectives: 18.6 us -> none  [sum_at_owner(): pieces = lax.all_to_all(split_up(array, dim, size), axis, 0, 0, tiled=True)]
    all_to_all x4 -> x0, starting transfers between devices: 17.4 us -> none  [the longest x1 6.75 us: side_by_side(): lax.all_to_all(both, axis, split_axis=split_dim, concat_axis=concat_dim,...]
    dot_general x13 -> x0, matrix products: 14.1 us -> none  [the longest x1 3.37 us: attend(): jnp.einsum('shd,shld->shl', queries, key_cache, preferred_element_type=jn...]
    reduce_sum x9 -> x0, other arithmetic: 1.26 us -> none  [the longest x1 0.34 us: attend(): denom_sum = jnp.sum(expo_terms, axis=-1) + own_expo]
  transfers between devices with their start and end apart: 4 -> 0, of which waited for: 4 -> 0; matrix products, arithmetic and copies ran while one was open for 1% -> 0% of each run, Pallas kernels for 0% -> 0%
where the time goes in v1:
time: 68.2 us; the launch traced here: 67.4 us
  Pallas kernels  46.1 us (68%)
  local copies, waits for them, and re-layouts  20.6 us (30%)
    pallas_call x1, Pallas kernels, body(): pl.pallas_call(kernel, out_shape=(jax.ShapeDtypeStruct((N, HD), BF), jax....  46.1 us
    unnamed x42, local copies, waits for them, and re-layouts  20.6 us

profile of v1, /device:TPU:1, one launch (start us, length us, event | category | flops | bytes accessed | tf_op | source)
XLA Modules:
  0.0 67.4 jit_solution(7608640635419922233)
XLA Ops:
  0.6 0.7 %copy.28.group_ids = s32[16,1]{1,0:T(8,128)S(1)} copy(s32[16,1]{0,1:T(1,128)} %param.36) | data formatting | bytes 128 | tf_op args[13]
  1.4 0.8 %copy.29.inner_ids = s32[16,2]{1,0:T(8,128)S(1)} copy(s32[16,2]{0,1:T(2,128)} %param.37) | data formatting | bytes 256 | tf_op args[14]
  2.1 0.8 %copy.30.pair_logits = f32[16,2]{1,0:T(8,128)S(1)} copy(f32[16,2]{0,1:T(2,128)} %param.39) | data formatting | bytes 256 | tf_op args[16]
  2.9 1.1 %copy.27.w_forget = bf16[2048,16]{1,0:T(8,128)(2,1)S(1)} copy(bf16[2048,16]{0,1:T(8,128)(2,1)} %param.32) | data formatting | bytes 131072 | tf_op args[9]
  4.0 0.0 copy-start
  4.0 1.0 %copy-done = bf16[2048,128]{1,0:T(8,128)(2,1)S(1)} copy-done((bf16[2048,128]{1,0:T(8,128)(2,1)S(1)}, bf16[2048,128]{1,0:T(8,128)(2,1)}, u32[]{:S(2)}) %copy-start) | copy-done | bytes 524312
  5.0 0.0 copy-start.1
  5.0 1.0 %copy-done.1 = bf16[2048,128]{1,0:T(8,128)(2,1)S(1)} copy-done((bf16[2048,128]{1,0:T(8,128)(2,1)S(1)}, bf16[2048,128]{1,0:T(8,128)(2,1)}, u32[]{:S(2)}) %copy-start.1) | copy-done | bytes 524312
  6.1 0.0 copy-start.2
  6.1 1.0 %copy-done.2 = bf16[2048,128]{1,0:T(8,128)(2,1)S(1)} copy-done((bf16[2048,128]{1,0:T(8,128)(2,1)S(1)}, bf16[2048,128]{1,0:T(8,128)(2,1)}, u32[]{:S(2)}) %copy-start.2) | copy-done | bytes 524312
  7.1 0.0 copy-start.3
  7.1 1.0 %copy-done.3 = bf16[128,2048]{1,0:T(8,128)(2,1)S(1)} copy-done((bf16[128,2048]{1,0:T(8,128)(2,1)S(1)}, bf16[128,2048]{1,0:T(8,128)(2,1)}, u32[]{:S(2)}) %copy-start.3) | copy-done | bytes 524312
  8.2 0.0 copy-start.4
  8.2 1.0 %copy-done.4 = bf16[1,2048,128]{2,1,0:T(8,128)(2,1)S(1)} copy-done((bf16[1,2048,128]{2,1,0:T(8,128)(2,1)S(1)}, bf16[1,2048,128]{2,1,0:T(8,128)(2,1)}, u32[]{:S(2)}) %copy-start.4) | copy-done | bytes 524312
  9.2 0.0 copy-start.5
  9.2 1.0 %copy-done.5 = bf16[1,2048,128]{2,1,0:T(8,128)(2,1)S(1)} copy-done((bf16[1,2048,128]{2,1,0:T(8,128)(2,1)S(1)}, bf16[1,2048,128]{2,1,0:T(8,128)(2,1)}, u32[]{:S(2)}) %copy-start.5) | copy-done | bytes 524312
  10.2 1.0 %copy-done.6 = bf16[1,128,2048]{2,1,0:T(8,128)(2,1)S(1)} copy-done((bf16[1,128,2048]{2,1,0:T(8,128)(2,1)S(1)}, bf16[1,128,2048]{2,1,0:T(8,128)(2,1)}, u32[]{:S(2)}) %copy-start.6) | copy-done | bytes 524312
  11.3 1.0 %copy-done.7 = bf16[2048,128]{1,0:T(8,128)(2,1)S(1)} copy-done((bf16[2048,128]{1,0:T(8,128)(2,1)S(1)}, bf16[2048,128]{1,0:T(8,128)(2,1)}, u32[]{:S(2)}) %copy-start.7) | copy-done | bytes 524312
  12.3 1.0 %copy-done.8 = bf16[128,2048]{1,0:T(8,128)(2,1)S(1)} copy-done((bf16[128,2048]{1,0:T(8,128)(2,1)S(1)}, bf16[128,2048]{1,0:T(8,128)(2,1)}, u32[]{:S(2)}) %copy-start.8) | copy-done | bytes 524312
  13.4 0.8 %copy-done.9 = f32[16,1,1024]{2,1,0:T(1,128)S(1)} copy-done((f32[16,1,1024]{2,1,0:T(1,128)S(1)}, f32[16,1,1024]{2,1,0:T(1,128)}, u32[]{:S(2)}) %copy-start.9) | copy-done | bytes 65560
  14.2 0.7 %copy-done.10 = f32[2048]{0:T(1024)S(1)} copy-done((f32[2048]{0:T(1024)S(1)}, f32[2048]{0:T(1024)}, u32[]{:S(2)}) %copy-start.10) | copy-done | bytes 8216
  14.9 0.7 %copy-done.11 = f32[2048]{0:T(1024)S(1)} copy-done((f32[2048]{0:T(1024)S(1)}, f32[2048]{0:T(1024)}, u32[]{:S(2)}) %copy-start.11) | copy-done | bytes 8216
  15.6 0.7 %copy-done.12 = bf16[16,128]{1,0:T(8,128)(2,1)S(1)} copy-done((bf16[16,128]{1,0:T(8,128)(2,1)S(1)}, bf16[16,128]{1,0:T(8,128)(2,1)}, u32[]{:S(2)}) %copy-start.12) | copy-done | bytes 4120
  16.3 0.7 copy-done.13
  17.0 0.7 copy-done.14
  17.6 0.7 copy-done.15
  18.3 0.7 copy-done.16
  18.9 46.1 %shard_map.246 = (bf16[16,128]{1,0:T(8,128)(2,1)S(1)}, bf16[16,128]{1,0:T(8,128)(2,1)S(1)}, bf16[16,128]{1,0:T(8,128)(2,1)S(1)}, f32[16,1]{1,0:T(8,128)S(1)}) custom-call(bf16[16,128]{1,0:T(8,128)(2,1)S(1)} %copy-done.12, bf16[16,1,1024,128]{3,2,1,0:T(8,128)(2,1)} %key_cache.1, bf16[16,1,1024,128]{3,2,1,0:T(8,128)(2,1)} %value_cache.1, ...), custom_call_target="tpu_custom_call" | custom-call | tf_op jit(solution)/shard_map/pallas_call | solution.py:300
  65.0 0.6 copy.31
  65.6 0.6 copy.35
  66.2 0.6 copy.36
  66.8 0.6 copy.37
  (11 shorter events, 0.0 us)
Async XLA Ops:
  4.0 1.0 %copy-start = (bf16[2048,128]{1,0:T(8,128)(2,1)S(1)}, bf16[2048,128]{1,0:T(8,128)(2,1)}, u32[]{:S(2)}) copy-start(bf16[2048,128]{1,0:T(8,128)(2,1)} %w_query.1) | copy-start | bytes 1572868
  5.0 1.0 %copy-start.1 = (bf16[2048,128]{1,0:T(8,128)(2,1)S(1)}, bf16[2048,128]{1,0:T(8,128)(2,1)}, u32[]{:S(2)}) copy-start(bf16[2048,128]{1,0:T(8,128)(2,1)} %w_key.1) | copy-start | bytes 1572868
  6.1 1.0 %copy-start.2 = (bf16[2048,128]{1,0:T(8,128)(2,1)S(1)}, bf16[2048,128]{1,0:T(8,128)(2,1)}, u32[]{:S(2)}) copy-start(bf16[2048,128]{1,0:T(8,128)(2,1)} %w_value.1) | copy-start | bytes 1572868
  7.1 1.0 %copy-start.3 = (bf16[128,2048]{1,0:T(8,128)(2,1)S(1)}, bf16[128,2048]{1,0:T(8,128)(2,1)}, u32[]{:S(2)}) copy-start(bf16[128,2048]{1,0:T(8,128)(2,1)} %w_attn_out.1) | copy-start | bytes 1572868
  8.2 1.0 %copy-start.4 = (bf16[1,2048,128]{2,1,0:T(8,128)(2,1)S(1)}, bf16[1,2048,128]{2,1,0:T(8,128)(2,1)}, u32[]{:S(2)}) copy-start(bf16[1,2048,128]{2,1,0:T(8,128)(2,1)} %w_gate.1) | copy-start | bytes 1572868
  9.2 1.0 %copy-start.5 = (bf16[1,2048,128]{2,1,0:T(8,128)(2,1)S(1)}, bf16[1,2048,128]{2,1,0:T(8,128)(2,1)}, u32[]{:S(2)}) copy-start(bf16[1,2048,128]{2,1,0:T(8,128)(2,1)} %w_up.1) | copy-start | bytes 1572868
  10.2 1.0 %copy-start.6 = (bf16[1,128,2048]{2,1,0:T(8,128)(2,1)S(1)}, bf16[1,128,2048]{2,1,0:T(8,128)(2,1)}, u32[]{:S(2)}) copy-start(bf16[1,128,2048]{2,1,0:T(8,128)(2,1)} %w_down.1) | copy-start | bytes 1572868
  11.3 1.0 %copy-start.7 = (bf16[2048,128]{1,0:T(8,128)(2,1)S(1)}, bf16[2048,128]{1,0:T(8,128)(2,1)}, u32[]{:S(2)}) copy-start(bf16[2048,128]{1,0:T(8,128)(2,1)} %w_din.1) | copy-start | bytes 1572868
  12.3 1.0 %copy-start.8 = (bf16[128,2048]{1,0:T(8,128)(2,1)S(1)}, bf16[128,2048]{1,0:T(8,128)(2,1)}, u32[]{:S(2)}) copy-start(bf16[128,2048]{1,0:T(8,128)(2,1)} %w_dout.1) | copy-start | bytes 1572868
  13.4 0.8 %copy-start.9 = (f32[16,1,1024]{2,1,0:T(1,128)S(1)}, f32[16,1,1024]{2,1,0:T(1,128)}, u32[]{:S(2)}) copy-start(f32[16,1,1024]{2,1,0:T(1,128)} %gate_totals.1) | copy-start | bytes 196612
  14.2 0.7 %copy-start.10 = (f32[2048]{0:T(1024)S(1)}, f32[2048]{0:T(1024)}, u32[]{:S(2)}) copy-start(f32[2048]{0:T(1024)} %param.28) | copy-start | bytes 24580
  14.9 0.7 %copy-start.11 = (f32[2048]{0:T(1024)S(1)}, f32[2048]{0:T(1024)}, u32[]{:S(2)}) copy-start(f32[2048]{0:T(1024)} %param.35) | copy-start | bytes 24580
  15.6 0.7 %copy-start.12 = (bf16[16,128]{1,0:T(8,128)(2,1)S(1)}, bf16[16,128]{1,0:T(8,128)(2,1)}, u32[]{:S(2)}) copy-start(bf16[16,128]{1,0:T(8,128)(2,1)} %tokens.1) | copy-start | bytes 12292
  16.3 0.7 copy-start.13
  17.0 0.7 copy-start.14
  17.6 0.7 copy-start.15
  18.3 0.7 copy-start.16

commit v2 on v1

--- a/solution.py
+++ b/solution.py
@@ -139,20 +139,19 @@
 
     for copy in c_route:
         copy.wait()
-    gid = gid_v[...]
+    gid = column_of(gid_v[...])
     choose = (gid == iota((N, N), 1)).astype(F32)
     lower = (iota((N, N), 1) < iota((N, N), 0)).astype(F32)
     before = dot(lower.astype(BF), choose.astype(BF))
     slot_of = gid * 2 + jnp.sum(before * choose, axis=1, keepdims=True).astype(jnp.int32)
-    first = sigmoid(pl_v[:, 0:1] - pl_v[:, 1:2])
-    prob = column_of(gp_v[...])
-    share0, share1 = prob * first, prob * (1.0 - first)
+    first = sigmoid(pl_v[0:1, :] - pl_v[1:2, :])
+    share0, share1 = gp_v[...] * first, gp_v[...] * (1.0 - first)
     expert = tp * HD // FFE
     inner = inn_v[...]
-    spread = jnp.where(inner[:, 0:1] == expert, share0, 0.0) + jnp.where(
-        inner[:, 1:2] == expert, share1, 0.0
-    )
-    spread = spread.astype(BF).astype(F32)
+    spread = jnp.where(inner[0:1, :] == expert, share0, 0.0) + jnp.where(
+        inner[1:2, :] == expert, share1, 0.0
+    )
+    spread = column_of(spread.astype(BF).astype(F32))
     spread_k = jnp.concatenate([spread] * KB, axis=0)
     slot_k = jnp.concatenate([slot_of] * KB, axis=0)
     rows, cols = iota((KB * N, 256), 0), iota((KB * N, 256), 1)
@@ -174,7 +173,7 @@
     toks = tok_all[...].astype(F32)
     normed = (toks * rms(toks) * ag_v[...]).astype(BF)
     qkv = dot(normed, wqkv[...])
-    fg = dot(normed, wf[...])
+    fg = dot(normed, wf[...], ((1,), (1,)))
     zq, zk = qkv[:, 0:HD], qkv[:, HD : 2 * HD]
     q = (zq * rms(zq)).astype(BF)
     new_k = (zk * rms(zk)).astype(BF)
@@ -194,7 +193,8 @@
     entry = iota((N, L), 1)
     last = jnp.sum(jnp.where(entry == length - 1, gt, 0.0), axis=1, keepdims=True)
     current = last + log_gate
-    gates_v[...] = current
+    same = iota((N, N), 0) == iota((N, N), 1)
+    gates_v[...] = jnp.sum(jnp.where(same, jnp.broadcast_to(current, (N, N)), 0.0), axis=0, keepdims=True)
     c_gates = pltpu.make_async_copy(gates_v, o_gates, osem.at[2])
     c_gates.start()
     o_copies.append(c_gates)
@@ -303,36 +303,36 @@
             jax.ShapeDtypeStruct((N, HD), BF),
             jax.ShapeDtypeStruct((N, HD), BF),
             jax.ShapeDtypeStruct((N, HD), BF),
-            jax.ShapeDtypeStruct((N, 1), F32),
+            jax.ShapeDtypeStruct((1, N), F32),
         ),
         in_specs=[any_space] * 23,
         out_specs=[any_space] * 4,
         scratch_shapes=[
-            vmem((L, D), BF), vmem((L, D), BF), vmem((D, 3 * HD), BF), vmem((D, N), BF),
+            vmem((L, D), BF), vmem((L, D), BF), vmem((D, 3 * HD), BF), vmem((N, D), BF),
             vmem((HD, D), BF), vmem((D, 2 * HD), BF), vmem((HD, D), BF), vmem((D, HD), BF),
             vmem((HD, D), BF), vmem((N, 1, L), F32), vmem((1, N), jnp.int32), vmem((1, D), F32),
-            vmem((1, N), F32), vmem((1, D), F32), vmem((N, 1), jnp.int32),
-            vmem((N, 2), jnp.int32), vmem((1, N), F32), vmem((N, 2), F32),
+            vmem((1, N), F32), vmem((1, D), F32), vmem((1, N), jnp.int32),
+            vmem((2, N), jnp.int32), vmem((1, N), F32), vmem((2, N), F32),
             vmem((N, D), BF), vmem((1, D), F32), vmem((256, KB * N), BF), vmem((KB * N, 256), BF),
             vmem((N, D), BF), vmem((N, N, HD), BF), vmem((N, D), BF), vmem((256, 256), BF),
             vmem((256, 256), BF), vmem((KB * N, 256), F32), vmem((256, 256), BF),
             vmem((256, 256), BF), vmem((N, N, HD), BF), vmem((N, N, HD), BF),
-            vmem((N, HD), BF), vmem((N, HD), BF), vmem((N, 1), F32), vmem((N, HD), BF),
+            vmem((N, HD), BF), vmem((N, HD), BF), vmem((1, N), F32), vmem((N, HD), BF),
             pltpu.SemaphoreType.DMA((64,)), pltpu.SemaphoreType.DMA((7, N)),
             pltpu.SemaphoreType.DMA((7, N)), pltpu.SemaphoreType.DMA((4,)),
         ],
         compiler_params=pltpu.CompilerParams(
-            collective_id=0, has_side_effects=True, vmem_limit_bytes=48 * 1024 * 1024
+            collective_id=0, has_side_effects=True, vmem_limit_bytes=67_043_328
         ),
     )(
         tokens, key_cache, value_cache, gate_totals, lengths.reshape(1, N),
-        attn_gain.reshape(1, D), w_query, w_key, w_value, w_forget, forget_bias.reshape(1, N),
-        w_attn_out, moe_gain.reshape(1, D), group_ids, inner_ids, group_prob.reshape(1, N),
-        pair_logits, w_expert_gate, w_expert_up, w_expert_down, w_dense_in, w_dense_out,
+        attn_gain.reshape(1, D), w_query, w_key, w_value, w_forget.T, forget_bias.reshape(1, N),
+        w_attn_out, moe_gain.reshape(1, D), group_ids.T, inner_ids.T,
+        group_prob.reshape(1, N), pair_logits.T, w_expert_gate, w_expert_up, w_expert_down, w_dense_in, w_dense_out,
         dense_gate.reshape(1, HD),
     )
     layer, keys, values, gates = outs
-    return (layer, keys.reshape(N, 1, HD), values.reshape(N, 1, HD), gates)
+    return (layer, keys.reshape(N, 1, HD), values.reshape(N, 1, HD), gates.reshape(N, 1))
 
 
 def solution(mesh):

time: 68.2 us -> 52.2 us (0.77)
  local copies, waits for them, and re-layouts: 20.6 us -> 4.94 us
    unnamed x42 -> x4, local copies, waits for them, and re-layouts: 20.6 us -> 4.94 us
where the time goes in v2:
time: 52.2 us; the launch traced here: 52 us
  Pallas kernels  46.4 us (89%)
  local copies, waits for them, and re-layouts  4.94 us (9%)
  between operations  0.65 us (1%)
    pallas_call x1, Pallas kernels, body(): pl.pallas_call(kernel, out_shape=(jax.ShapeDtypeStruct((N, HD), BF), jax....  46.4 us
    unnamed x4, local copies, waits for them, and re-layouts  4.94 us

profile of v2, /device:TPU:1, one launch (start us, length us, event | category | flops | bytes accessed | tf_op | source)
XLA Modules:
  0.0 52.0 jit_solution(7161467084295368866)
XLA Ops:
  0.6 46.4 %shard_map.246 = (bf16[16,128]{1,0:T(8,128)(2,1)}, bf16[16,128]{1,0:T(8,128)(2,1)}, bf16[16,128]{1,0:T(8,128)(2,1)}, f32[1,16]{1,0:T(1,128)}) custom-call(bf16[16,128]{1,0:T(8,128)(2,1)} %tokens.1, bf16[16,1,1024,128]{3,2,1,0:T(8,128)(2,1)} %key_cache.1, bf16[16,1,1024,128]{3,2,1,0:T(8,128)(2,1)} %value_cache.1, f32[16,1,1024]{2,1,0:T(1,128)} %gate_totals.1, ...), custom_call_target="tpu_custom_call" | custom-call | tf_op jit(solution)/shard_map/pallas_call | solution.py:300
  47.0 1.3 %copy.31 = bf16[16,128]{1,0:T(8,128)(2,1)} copy(bf16[16,128]{1,0:T(8,128)(2,1)} %get-tuple-element.16) | data formatting | bytes 8192
  48.3 1.3 %copy.32 = bf16[16,1,128]{2,0,1:T(8,128)(2,1)} copy(bf16[16,1,128]{2,0,1:T(8,128)(2,1)} %bitcast.17) | data formatting | bytes 8192
  49.6 1.3 %copy.33 = bf16[16,1,128]{2,0,1:T(8,128)(2,1)} copy(bf16[16,1,128]{2,0,1:T(8,128)(2,1)} %bitcast.16) | data formatting | bytes 8192
  50.8 1.1 %copy.34 = f32[16,1]{0,1:T(1,128)} copy(f32[16,1]{0,1:T(1,128)} %bitcast.25) | data formatting | bytes 128

commit v3 on v2

--- a/solution.py
+++ b/solution.py
@@ -13,7 +13,6 @@
 D = N * HD
 L = 1024
 FFE = 512
-KB = D // 256
 F32 = jnp.float32
 BF = jnp.bfloat16
 TP_ORDER = (8, 9, 7, 6, 10, 5, 11, 4, 12, 3, 13, 2, 14, 15, 1)
@@ -48,15 +47,25 @@
     w_gate, w_up, w_down, w_din, w_dout, dense_gate,
     o_layer, o_keys, o_values, o_gates,
     k_v, v_v, wqkv, wf, wo, wgu, wdn, wdi, wdo, gt_v, len_v, ag_v, fb_v, mg_v, gid_v, inn_v,
-    gp_v, pl_v, tok_all, dg_all, p_v, pt_v, part2, recv2, res_all, send4, recv4, dpart,
+    gp_v, pl_v, tok_all, dg_all, part2, recv2, res_all, send4, recv4, dpart,
     send5, recv5, part6, recv6, keys_v, vals_v, gates_v, lay_v,
     lsem, ssem, rsem, osem,
 ):
     ep = lax.axis_index("ep")
     tp = lax.axis_index("tp")
     tcol = pl.ds(pl.multiple_of(tp * HD, HD), HD)
-    erow = pl.ds(pl.multiple_of(ep * N, N), N)
-
+    erow = pl.ds(pl.multiple_of(ep * 2, 2), 2)
+
+    count = [0]
+
+    def local(src, dst):
+        copy = pltpu.make_async_copy(src, dst, lsem.at[count[0]])
+        count[0] += 1
+        copy.start()
+        return copy
+
+    c_tok = local(tokens, tok_all.at[:, tcol])
+    c_dg = local(dense_gate, dg_all.at[:, tcol])
     barrier = pltpu.get_barrier_semaphore()
     for off in range(1, N):
         pl.semaphore_signal(
@@ -65,17 +74,6 @@
         pl.semaphore_signal(
             barrier, inc=1, device_id={"ep": lax.rem(ep + off, N)}, device_id_type=MESH
         )
-
-    count = [0]
-
-    def local(src, dst):
-        copy = pltpu.make_async_copy(src, dst, lsem.at[count[0]])
-        count[0] += 1
-        copy.start()
-        return copy
-
-    c_tok = local(tokens, tok_all.at[:, tcol])
-    c_dg = local(dense_gate, dg_all.at[:, tcol])
     c_route = [
         local(group_ids, gid_v), local(inner_ids, inn_v), local(group_prob, gp_v),
         local(pair_logits, pl_v),
@@ -132,18 +130,28 @@
         return lambda peer: ref.at[:, pl.ds(pl.multiple_of(peer * HD, HD), HD)]
 
     def ep_rows(ref):
-        return lambda peer: ref.at[pl.ds(pl.multiple_of(peer * N, N), N), :]
+        return lambda peer: ref.at[pl.ds(pl.multiple_of(peer * 2, 2), 2), :]
 
     def slots(ref):
         return lambda peer: ref.at[peer]
 
+    c_tok.wait()
+    pl.semaphore_wait(barrier, 2 * (N - 1))
+    push(0, "tp", TP_ORDER, lambda peer: tok_all.at[:, tcol], tok_all.at[:, tcol])
+    c_dg.wait()
+    push(1, "tp", TP_ORDER, lambda peer: dg_all.at[:, tcol], dg_all.at[:, tcol])
+
     for copy in c_route:
         copy.wait()
-    gid = column_of(gid_v[...])
-    choose = (gid == iota((N, N), 1)).astype(F32)
-    lower = (iota((N, N), 1) < iota((N, N), 0)).astype(F32)
-    before = dot(lower.astype(BF), choose.astype(BF))
-    slot_of = gid * 2 + jnp.sum(before * choose, axis=1, keepdims=True).astype(jnp.int32)
+    gid = gid_v[...]
+    gid_col = column_of(gid)
+    same = gid_col == jnp.broadcast_to(gid, (N, N))
+    earlier = iota((N, N), 0) < iota((N, N), 1)
+    rank = jnp.sum((same & earlier).astype(jnp.int32), axis=0, keepdims=True)
+    later = iota((N, N), 1) < iota((N, N), 0)
+    rank_col = jnp.sum((same & later).astype(jnp.int32), axis=1, keepdims=True)
+    send_map = (gid * 2 + rank == iota((2 * N, N), 0)).astype(F32).astype(BF)
+    back_map = (gid_col * 2 + rank_col == iota((N, 2 * N), 1)).astype(F32).astype(BF)
     first = sigmoid(pl_v[0:1, :] - pl_v[1:2, :])
     share0, share1 = gp_v[...] * first, gp_v[...] * (1.0 - first)
     expert = tp * HD // FFE
@@ -152,22 +160,13 @@
         inner[1:2, :] == expert, share1, 0.0
     )
     spread = column_of(spread.astype(BF).astype(F32))
-    spread_k = jnp.concatenate([spread] * KB, axis=0)
-    slot_k = jnp.concatenate([slot_of] * KB, axis=0)
-    rows, cols = iota((KB * N, 256), 0), iota((KB * N, 256), 1)
-    pt = ((slot_k == cols // KB) & (rows // N == lax.rem(cols, KB))).astype(F32)
-    pt_v[...] = pt.astype(BF)
-    p_v[...] = pt.T.astype(BF)
-
-    c_tok.wait()
-    c_dg.wait()
-    pl.semaphore_wait(barrier, 2 * (N - 1))
-    push(0, "tp", TP_ORDER, lambda peer: tok_all.at[:, tcol], tok_all.at[:, tcol])
-    push(1, "tp", TP_ORDER, lambda peer: dg_all.at[:, tcol], dg_all.at[:, tcol])
-
     for copy in c_small + c_qkv:
         copy.wait()
     length = column_of(len_v[...])
+    gt = gt_v[...].reshape(N, L)
+    entry = iota((N, L), 1)
+    live = entry < length
+    last = jnp.sum(jnp.where(entry == length - 1, gt, 0.0), axis=1, keepdims=True)
     arrive(0, "tp", TP_ORDER, tp_cols(tok_all))
 
     toks = tok_all[...].astype(F32)
@@ -189,9 +188,6 @@
     pre = fg + fb_v[...]
     pre = jnp.sum(jnp.where(iota((N, N), 1) == tp, pre, 0.0), axis=1, keepdims=True)
     log_gate = jnp.minimum(pre, 0.0) - jnp.log(1.0 + jnp.exp(-jnp.abs(pre)))
-    gt = gt_v[...].reshape(N, L)
-    entry = iota((N, L), 1)
-    last = jnp.sum(jnp.where(entry == length - 1, gt, 0.0), axis=1, keepdims=True)
     current = last + log_gate
     same = iota((N, N), 0) == iota((N, N), 1)
     gates_v[...] = jnp.sum(jnp.where(same, jnp.broadcast_to(current, (N, N)), 0.0), axis=0, keepdims=True)
@@ -209,7 +205,6 @@
         [dot(q_wide, k_v[c : c + 256, :], ((1,), (1,))) for c in range(0, L, 256)], axis=1
     )
     scores = scores * scale + current - gt
-    live = entry < length
     scores = jnp.where(live, scores, FLOOR)
     own = jnp.sum(q.astype(F32) * new_k.astype(F32), axis=1, keepdims=True) * scale
     peak = jnp.maximum(jnp.max(scores, axis=1, keepdims=True), own)
@@ -245,39 +240,26 @@
 
     res = res_all[...].astype(F32)
     moe_in = (res * rms(res) * mg_v[...]).astype(BF)
-    blocks = jnp.concatenate([moe_in[:, k * 256 : (k + 1) * 256] for k in range(KB)], axis=0)
-    send4[...] = dot(p_v[...], blocks).astype(BF)
+    send4[...] = dot(send_map, moe_in).astype(BF)
     push(4, "ep", EP_ORDER, ep_rows(send4), recv4.at[erow, :])
-    recv4[erow, :] = send4[erow, :]
 
     hidden = dot(moe_in, wdi[...])
     hidden = (hidden * sigmoid(hidden)).astype(BF)
-    dense = dot(hidden, wdo[...]) * dense_scale
-    for k in range(KB):
-        dpart[k * N : (k + 1) * N, :] = dense[:, k * 256 : (k + 1) * 256]
-
-    rows, cols = iota((256, 256), 0), iota((256, 256), 1)
-    regroup = (lax.rem(rows, 32) * KB + rows // 32 == cols).astype(F32).astype(BF)
-    ungroup = (lax.rem(cols, 32) * KB + cols // 32 == rows).astype(F32).astype(BF)
+    dpart[...] = dot(hidden, wdo[...]) * dense_scale
+
     arrive(4, "ep", EP_ORDER, ep_rows(recv4))
-    xs = dot(regroup, recv4[...]).astype(BF)
-    x = jnp.concatenate([xs[k * 32 : (k + 1) * 32, :] for k in range(KB)], axis=1)
+    mine = iota((2 * N, D), 0) // 2 == ep
+    x = jnp.where(mine, send4[...], recv4[...])
     gu = dot(x, wgu[...])
     g, u = gu[:, 0:HD], gu[:, HD : 2 * HD]
     h = (g * sigmoid(g) * u).astype(BF)
-    y = dot(h, wdn[...]).astype(BF)
-    ys = jnp.concatenate([y[:, k * 256 : (k + 1) * 256] for k in range(KB)], axis=0)
-    send5[...] = dot(ungroup, ys).astype(BF)
+    send5[...] = dot(h, wdn[...]).astype(BF)
     push(5, "ep", EP_ORDER, ep_rows(send5), recv5.at[erow, :])
-    recv5[erow, :] = send5[erow, :]
     arrive(5, "ep", EP_ORDER, ep_rows(recv5))
 
-    total = (dot(pt_v[...], recv5[...]) * spread_k + dpart[...]).astype(BF)
-    for t in range(N):
-        k, half = t // 2, t % 2
-        part6[t] = total[k * N : (k + 1) * N, half * HD : (half + 1) * HD]
-    push(6, "tp", TP_ORDER, slots(part6), recv6.at[tp])
-    recv6[tp] = part6[tp]
+    part6[...] = (dot(back_map, jnp.where(mine, send5[...], recv5[...])) * spread + dpart[...]).astype(BF)
+    push(6, "tp", TP_ORDER, tp_cols(part6), recv6.at[tp])
+    recv6[tp] = part6[:, tcol]
     own_res = res_all[:, tcol].astype(F32)
     arrive(6, "tp", TP_ORDER, slots(recv6))
     lay_v[...] = (own_res + jnp.sum(recv6[...].astype(F32), axis=0)).astype(BF)
@@ -287,6 +269,19 @@
     for copy in sends:
         copy.wait_send()
     for copy in o_copies:
+        copy.wait()
+
+
+def writer(*refs):
+    ins, outs, held, sem = refs[0:4], refs[4:8], refs[8:12], refs[12]
+    reads = [pltpu.make_async_copy(ins[i], held[i], sem.at[0, i]) for i in range(4)]
+    writes = [pltpu.make_async_copy(held[i], outs[i], sem.at[1, i]) for i in range(4)]
+    for copy in reads:
+        copy.start()
+    for read, write in zip(reads, writes):
+        read.wait()
+        write.start()
+    for copy in writes:
         copy.wait()
 
 
@@ -313,10 +308,9 @@
             vmem((HD, D), BF), vmem((N, 1, L), F32), vmem((1, N), jnp.int32), vmem((1, D), F32),
             vmem((1, N), F32), vmem((1, D), F32), vmem((1, N), jnp.int32),
             vmem((2, N), jnp.int32), vmem((1, N), F32), vmem((2, N), F32),
-            vmem((N, D), BF), vmem((1, D), F32), vmem((256, KB * N), BF), vmem((KB * N, 256), BF),
-            vmem((N, D), BF), vmem((N, N, HD), BF), vmem((N, D), BF), vmem((256, 256), BF),
-            vmem((256, 256), BF), vmem((KB * N, 256), F32), vmem((256, 256), BF),
-            vmem((256, 256), BF), vmem((N, N, HD), BF), vmem((N, N, HD), BF),
+            vmem((N, D), BF), vmem((1, D), F32), vmem((N, D), BF), vmem((N, N, HD), BF),
+            vmem((N, D), BF), vmem((2 * N, D), BF), vmem((2 * N, D), BF), vmem((N, D), F32),
+            vmem((2 * N, D), BF), vmem((2 * N, D), BF), vmem((N, D), BF), vmem((N, N, HD), BF),
             vmem((N, HD), BF), vmem((N, HD), BF), vmem((1, N), F32), vmem((N, HD), BF),
             pltpu.SemaphoreType.DMA((64,)), pltpu.SemaphoreType.DMA((7, N)),
             pltpu.SemaphoreType.DMA((7, N)), pltpu.SemaphoreType.DMA((4,)),
@@ -331,7 +325,14 @@
         group_prob.reshape(1, N), pair_logits.T, w_expert_gate, w_expert_up, w_expert_down, w_dense_in, w_dense_out,
         dense_gate.reshape(1, HD),
     )
-    layer, keys, values, gates = outs
+    layer, keys, values, gates = pl.pallas_call(
+        writer,
+        out_shape=[jax.ShapeDtypeStruct(o.shape, o.dtype) for o in outs],
+        in_specs=[any_space] * 4,
+        out_specs=[any_space] * 4,
+        scratch_shapes=[vmem(o.shape, o.dtype) for o in outs] + [pltpu.SemaphoreType.DMA((2, 4))],
+        compiler_params=pltpu.CompilerParams(vmem_limit_bytes=67_043_328),
+    )(*outs)
     return (layer, keys.reshape(N, 1, HD), values.reshape(N, 1, HD), gates.reshape(N, 1))
 
 

time: 52.2 us -> 48.2 us (0.923)
  local copies, waits for them, and re-layouts: 4.94 us -> 0 us
  Pallas kernels: 46.4 us -> 47.4 us
    unnamed x4 -> x0, local copies, waits for them, and re-layouts: 4.94 us -> none
    pallas_call x0 -> x1, Pallas kernels: none -> 1.35 us  [body(): pl.pallas_call(writer, out_shape=[jax.ShapeDtypeStruct(o.shape, o.dtype)...]
where the time goes in v3:
time: 48.2 us; the launch traced here: 48 us
  Pallas kernels  47.4 us (98%)
  between operations  0.65 us (1%)
    pallas_call x1, Pallas kernels, body(): pl.pallas_call(kernel, out_shape=(jax.ShapeDtypeStruct((N, HD), BF), jax....  46 us
    pallas_call x1, Pallas kernels, body(): pl.pallas_call(writer, out_shape=[jax.ShapeDtypeStruct(o.shape, o.dtype)...  1.35 us

profile of v3, /device:TPU:1, one launch (start us, length us, event | category | flops | bytes accessed | tf_op | source)
XLA Modules:
  0.0 48.0 jit_solution(16378987469637552462)
XLA Ops:
  0.6 46.0 %shard_map.246 = (bf16[16,128]{1,0:T(8,128)(2,1)}, bf16[16,128]{1,0:T(8,128)(2,1)}, bf16[16,128]{1,0:T(8,128)(2,1)}, f32[1,16]{1,0:T(1,128)}) custom-call(bf16[16,128]{1,0:T(8,128)(2,1)} %tokens.1, bf16[16,1,1024,128]{3,2,1,0:T(8,128)(2,1)} %key_cache.1, bf16[16,1,1024,128]{3,2,1,0:T(8,128)(2,1)} %value_cache.1, f32[16,1,1024]{2,1,0:T(1,128)} %gate_totals.1, ...), custom_call_target="tpu_custom_call" | custom-call | tf_op jit(solution)/shard_map/pallas_call | solution.py:295
  46.7 1.4 %shard_map.247 = (bf16[16,128]{1,0:T(8,128)(2,1)}, bf16[16,128]{1,0:T(8,128)(2,1)}, bf16[16,128]{1,0:T(8,128)(2,1)}, f32[1,16]{1,0:T(1,128)}) custom-call(bf16[16,128]{1,0:T(8,128)(2,1)} %get-tuple-element.12.refs_0_, bf16[16,128]{1,0:T(8,128)(2,1)} %get-tuple-element.13.refs_1_, bf16[16,128]{1,0:T(8,128)(2,1)} %get-tuple-element.14.refs_2_, ...), custom_call_target="tpu_custom_call" | custom-call | tf_op jit(solution)/shard_map/pallas_call | solution.py:328
